TPU v7x, 32 devices: a whole 2x2x4 slice. The times are simulated.
32 devices in a mesh: ep: 8 (over z, x), tp: 4 (over y, core).
Axes of the slice: x: 2, y: 2, z: 4, core: 2. Of those that a mesh axis runs over, the one named last changes fastest.
Arguments:
- tokens: bfloat16 [32, 2048], P('ep'), may hold values from -6 to 6
- attn_gain: bfloat16 [2048], replicated, may hold values from 0.099609375 to 1.8984375
- ffn_gain: bfloat16 [2048], replicated, may hold values from 0.099609375 to 1.8984375
- w_query: bfloat16 [2048, 2048], P(None, 'tp'), may hold values from -0.125 to 0.125
- w_key: bfloat16 [2048, 256], replicated, may hold values from -0.125 to 0.125
- w_value: bfloat16 [2048, 256], replicated, may hold values from -0.125 to 0.125
- w_forget: bfloat16 [2048, 32], replicated, may hold values from -0.125 to 0.125
- forget_bias: float32 [32], replicated, may hold values from -1 to 3
- w_out: bfloat16 [2048, 2048], P(None, 'tp'), may hold values from -0.375 to 0.375
- cache_keys: bfloat16 [32, 2048, 256], P(('ep', 'tp')), may hold values from -800 to 800
- cache_values: bfloat16 [32, 2048, 256], P(('ep', 'tp')), may hold values from -6 to 6
- cache_logcum: float32 [32, 32, 2048], P(('ep', 'tp')), as said below
- cache_len: int32 [32], P(('ep', 'tp')), may hold values from 256 to 2048
- route_group: int32 [32], P('ep'), may hold values from 0 to 3, as said below
- route_expert: int32 [32, 2], P('ep'), may hold values from 0 to 1, as said below
- route_weight: float32 [32, 2], P('ep'), may hold values from 0.2 to 1
- w_gate: bfloat16 [8, 2048, 2048], P('ep', None, 'tp'), may hold values from -0.125 to 0.125
- w_up: bfloat16 [8, 2048, 2048], P('ep', None, 'tp'), may hold values from -0.125 to 0.125
- w_down: bfloat16 [8, 2048, 2048], P('ep', None, 'tp'), may hold values from -0.125 to 0.125
Outputs:
- layer_out: bfloat16 [32, 2048], P('ep', 'tp')
Inputs may be any that keep to these rules, and one draw needn't show every extreme that they name: Expert groups. Among the 4 sequences of one index of ep no expert route_group * 2 + route_expert is named more than 3 times, and in every draw one expert is named exactly 3 times by the sequences of every index of ep. `route_expert`: the 2 numbers of a sequence differ. `cache_logcum`: each entry is the sum of the log forget gates of that head from the first cached position up to and including that position.
All inputs are finite; a program needn't handle non-finite values.
Results may differ from a plain program's by a relative error of at most 0.012.
The roundings to bfloat16 on the way count: a program that leaves them out, or rounds other values in their place, can miss the bound.
Values may be sent and summed in bfloat16 or wider, within the bound.
A program may use at most 64 MiB of HBM per device.

v0:
```python
import functools

import jax
import jax.numpy as jnp
from jax import lax
from jax.experimental import pallas as pl
from jax.experimental.pallas import tpu as pltpu
from jax.sharding import PartitionSpec as P

QUERY_HEAD_COUNT = 32
KV_HEADS = 4
HEAD = 64
GROUPS = 4
TOP = 2
PER_KV = QUERY_HEAD_COUNT // KV_HEADS
LANES = 128
NORM_EPSILON = 1e-06
MASKED_SCORE = -1e30
F32 = jnp.float32
BF16 = jnp.bfloat16
MESH = pl.DeviceIdType.MESH


def dot(a, b):
    return jnp.dot(a, b, preferred_element_type=F32)


def as_row(ref):
    block = ref[...].astype(F32)
    return jnp.concatenate([block[i : i + 1] for i in range(block.shape[0])], axis=1)


def each(count, body):
    if count <= 8:
        for step in range(count):
            body(step)
    else:

        @pl.loop(0, count)
        def _(step):
            body(step)


def kernel(
    n_ep,
    n_tp,
    tokens_hbm,
    attn_gain_hbm,
    ffn_gain_hbm,
    forget_bias_hbm,
    cache_len_hbm,
    route_group_hbm,
    route_expert_hbm,
    route_weight_hbm,
    wq_hbm,
    wk_hbm,
    wv_hbm,
    wf_hbm,
    wo_hbm,
    keys_hbm,
    values_hbm,
    logcum_hbm,
    wg_hbm,
    wu_hbm,
    wd_hbm,
    out,
    tokens,
    attn_gain,
    ffn_gain,
    forget_bias,
    cache_len,
    route_group,
    route_expert,
    route_weight,
    wq,
    wk,
    wv,
    wf,
    wo,
    keys,
    values,
    logcum,
    wg,
    wu,
    wd,
    q_send,
    q_recv,
    att_send,
    att_recv,
    att_rows,
    mix_send,
    mix_recv,
    hid_send,
    hid_recv,
    ret_send,
    ret_recv,
    load_sem,
    q_ssem,
    q_rsem,
    att_ssem,
    att_rsem,
    mix_ssem,
    mix_rsem,
    hid_ssem,
    hid_rsem,
    ret_ssem,
    ret_rsem,
    near_sem,
    gain_parts,
):
    ep = lax.axis_index("ep")
    tp = lax.axis_index("tp")
    pairs = n_tp // 2

    def tp_peer(offset):
        pair = lax.rem(tp // 2 + offset // 2, pairs)
        core = lax.rem(lax.rem(tp, 2) + offset % 2, 2)
        return pair * 2 + core

    def tp_source(offset):
        pair = lax.rem(tp // 2 + pairs - offset // 2, pairs)
        core = lax.rem(lax.rem(tp, 2) + offset % 2, 2)
        return pair * 2 + core

    def ep_peer(offset):
        return lax.rem(ep + offset, n_ep)

    def far_first(step, skip):
        return skip + lax.rem(step + n_ep // 2 - 2 * skip, n_ep - skip)

    loads = {}
    for index, (name, source, target) in enumerate(
        (
            ("tokens", tokens_hbm, tokens),
            ("attn_gain", attn_gain_hbm, attn_gain),
            ("ffn_gain", ffn_gain_hbm, ffn_gain),
            ("forget_bias", forget_bias_hbm, forget_bias),
            ("cache_len", cache_len_hbm, cache_len),
            ("route_group", route_group_hbm, route_group),
            ("route_expert", route_expert_hbm, route_expert),
            ("route_weight", route_weight_hbm, route_weight),
            ("wq", wq_hbm, wq),
            ("wk", wk_hbm, wk),
            ("wv", wv_hbm, wv),
            ("wf", wf_hbm, wf),
            ("logcum", logcum_hbm.at[0], logcum),
            ("keys", keys_hbm.at[0], keys),
            ("values", values_hbm.at[0], values),
            ("wo", wo_hbm, wo),
            ("wg", wg_hbm.at[0], wg),
            ("wu", wu_hbm.at[0], wu),
            ("wd", wd_hbm.at[0], wd),
        )
    ):
        loads[name] = pltpu.make_async_copy(source, target, load_sem.at[index])
    small = ("ffn_gain", "forget_bias", "cache_len", "route_group", "route_expert", "route_weight")
    for name in ("tokens", "attn_gain", "wq"):
        loads[name].start()

    barrier = pltpu.get_barrier_semaphore()
    pair, pair_count = ep // 2, n_ep // 2

    def signal_line(semaphore, distance):
        for step in (-distance, distance):

            @pl.when(jnp.logical_and(pair + step >= 0, pair + step < pair_count))
            def _(step=step):
                pl.semaphore_signal(
                    semaphore, inc=1, device_id=(ep + 2 * step, tp), device_id_type=MESH
                )

    def line_count(distance):
        before = (pair - distance >= 0).astype(jnp.int32)
        return before + (pair + distance < pair_count).astype(jnp.int32)

    for offset in range(1, n_tp):
        pl.semaphore_signal(barrier, inc=1, device_id=(ep, tp_peer(offset)), device_id_type=MESH)
    other = pair * 2 + 1 - lax.rem(ep, 2)
    pl.semaphore_signal(barrier, inc=1, device_id=(other, tp), device_id_type=MESH)
    signal_line(barrier, 1)
    for name in ("wk", "wv", "wf", *small, "logcum"):
        loads[name].start()

    rows = tokens.shape[0]
    width = wo.shape[1]
    depth = tokens.shape[1]
    length = keys.shape[0]
    loads["tokens"].wait()
    loads["attn_gain"].wait()
    stream = tokens[...].astype(F32)
    square = jnp.mean(stream * stream, axis=-1, keepdims=True)
    normed = (stream * lax.rsqrt(square + NORM_EPSILON) * as_row(attn_gain)).astype(BF16)

    loads["wq"].wait()
    query = dot(normed, wq[...]).astype(BF16).astype(F32)
    for name in ("keys", "values", "wo", "wg", "wu", "wd"):
        loads[name].start()
    for row in range(rows):
        q_send[row] = query[row : row + 1, :]
    pl.semaphore_wait(barrier, n_tp + line_count(1))

    def q_copy(offset):
        peer = tp_peer(offset)
        return pltpu.make_async_remote_copy(
            src_ref=q_send.at[peer],
            dst_ref=q_recv.at[tp],
            send_sem=q_ssem.at[offset],
            recv_sem=q_rsem.at[offset],
            device_id=(ep, peer),
            device_id_type=MESH,
        )

    q_copies = [q_copy(offset) for offset in range(1, n_tp)]
    for copy in q_copies:
        copy.start()
    q_recv[tp] = q_send[tp]

    def spread(index):
        if index == 1:
            pl.semaphore_wait(near_sem.at[0], 1)
        elif index:
            pl.semaphore_wait(near_sem.at[index - 1], line_count(2 ** (index - 2)))
        if index == 0:
            pl.semaphore_signal(
                near_sem.at[0], inc=1, device_id=(other, tp), device_id_type=MESH
            )
        elif index < near_sem.shape[0]:
            signal_line(near_sem.at[index], 2 ** (index - 1))

    spread(0)

    own = lax.broadcasted_iota(jnp.int32, (rows, 1), 0) == tp

    def own_row(values_all):
        return jnp.sum(jnp.where(own, values_all, 0.0), axis=0, keepdims=True)

    loads["wk"].wait()
    key_new = own_row(dot(normed, wk[...])).astype(BF16).astype(F32)
    loads["wv"].wait()
    value_new = own_row(dot(normed, wv[...])).astype(BF16).astype(F32)
    loads["wf"].wait()
    for name in small:
        loads[name].wait()
    heads = QUERY_HEAD_COUNT
    gates = lax.dot_general(
        wf[...], normed, (((1,), (1,)), ((), ())), preferred_element_type=F32
    )
    own_lane = lax.broadcasted_iota(jnp.int32, (1, rows), 1) == tp
    gate_sum = jnp.sum(jnp.where(own_lane, gates, 0.0), axis=1, keepdims=True)
    diagonal = lax.broadcasted_iota(jnp.int32, (heads, heads), 0) == lax.broadcasted_iota(
        jnp.int32, (heads, heads), 1
    )
    bias_sum = jnp.sum(jnp.where(diagonal, forget_bias[...], 0.0), axis=1, keepdims=True)
    log_gate = jax.nn.log_sigmoid(gate_sum + bias_sum)
    used = cache_len[0, 0]
    position = lax.broadcasted_iota(jnp.int32, (1, length), 1)
    loads["logcum"].wait()
    cum = logcum[...]
    latest = jnp.sum(jnp.where(position == used - 1, cum, 0.0), axis=1, keepdims=True)
    bias = jnp.where(position < used, (latest + log_gate) - cum, MASKED_SCORE)

    loads["keys"].wait()
    spread(1)
    for copy in q_copies:
        copy.wait_recv()

    span = PER_KV * HEAD
    q_row = jnp.concatenate([q_recv[source] for source in range(n_tp)], axis=1)
    row_of = lax.broadcasted_iota(jnp.int32, (PER_KV, span), 0)
    lane_of = lax.broadcasted_iota(jnp.int32, (PER_KV, span), 1) // HEAD
    half_of = lax.broadcasted_iota(jnp.int32, (PER_KV, LANES), 1) // HEAD
    zeros = jnp.zeros((PER_KV, LANES), F32)
    blocks = []
    for head in range(KV_HEADS):
        part = jnp.broadcast_to(q_row[:, head * span : (head + 1) * span], (PER_KV, span))
        part = jnp.where(row_of == lane_of, part, 0.0)
        fold = part[:, :LANES]
        for tile in range(1, span // LANES):
            fold = fold + part[:, tile * LANES : (tile + 1) * LANES]
        fold = fold + pltpu.roll(fold, HEAD, 1)
        fold = jnp.where(half_of == head % 2, fold, 0.0)
        tiles = [zeros] * (KV_HEADS * HEAD // LANES)
        tiles[head * HEAD // LANES] = fold
        blocks.append(jnp.concatenate(tiles, axis=1))
    q_heads = jnp.concatenate(blocks, axis=0)
    scale = HEAD ** (-0.5)
    own_score = jnp.sum(q_heads * key_new, axis=1, keepdims=True) * scale
    score = lax.dot_general(
        q_heads.astype(BF16), keys[...], (((1,), (1,)), ((), ())), preferred_element_type=F32
    )
    score = score * scale + bias
    peak = jnp.maximum(jnp.max(score, axis=1, keepdims=True), own_score)
    weight = jnp.exp(score - peak)
    own_weight = jnp.exp(own_score - peak)
    denominator = jnp.sum(weight, axis=1, keepdims=True) + own_weight
    loads["values"].wait()
    summed = dot(weight.astype(BF16), values[...])
    summed = summed + own_weight.astype(BF16).astype(F32) * value_new
    summed = summed / denominator
    kv_of = lax.broadcasted_iota(jnp.int32, (PER_KV, KV_HEADS * HEAD), 1) // HEAD
    folded = summed[:PER_KV]
    for head in range(1, KV_HEADS):
        folded = jnp.where(kv_of == head, summed[head * PER_KV : (head + 1) * PER_KV], folded)
    attended = folded.astype(BF16)
    att_send[...] = attended

    def att_copy(offset):
        return pltpu.make_async_remote_copy(
            src_ref=att_send,
            dst_ref=att_recv.at[tp],
            send_sem=att_ssem.at[offset],
            recv_sem=att_rsem.at[offset],
            device_id=(ep, tp_peer(offset)),
            device_id_type=MESH,
        )

    att_copies = [att_copy(offset) for offset in range(1, n_tp)]
    for copy in att_copies[::-1]:
        copy.start()
    att_recv[tp] = attended
    loads["wo"].wait()
    spread(2)
    for copy in att_copies:
        copy.wait_recv()
    for source in range(n_tp):
        arrived = att_recv[source].astype(F32)
        for tile in range(att_rows.shape[0]):
            att_rows[tile, source * PER_KV : (source + 1) * PER_KV] = arrived[
                :, tile * LANES : (tile + 1) * LANES
            ]
    left = jnp.concatenate(
        [
            att_rows[tile, pl.ds(j, n_tp, stride=PER_KV), :]
            for j in range(PER_KV)
            for tile in range(att_rows.shape[0])
        ],
        axis=1,
    ).astype(BF16)
    right = jnp.concatenate(
        [
            wo[head * span + j * HEAD : head * span + (j + 1) * HEAD, :]
            for j in range(PER_KV)
            for head in range(KV_HEADS)
        ],
        axis=0,
    )
    projected = dot(left, right)
    residual = tokens[:, pl.ds(pl.multiple_of(tp * width, LANES), width)].astype(F32)
    mixed = (residual + projected).astype(BF16)
    mix_send[...] = mixed

    for index in range(3, near_sem.shape[0] + 1):
        spread(index)

    def mix_copy(t_off, step):
        return pltpu.make_async_remote_copy(
            src_ref=mix_send,
            dst_ref=mix_recv.at[tp, ep],
            send_sem=mix_ssem.at[t_off],
            recv_sem=mix_rsem.at[t_off],
            device_id=(ep_peer(step), tp_peer(t_off)),
            device_id_type=MESH,
        )

    for t_off in range(0, n_tp, 2):
        skip = 0 if t_off else 1
        each(n_ep - skip, lambda step, t_off=t_off, skip=skip: mix_copy(t_off, far_first(step, skip)).start())
    mix_recv[tp, ep] = mixed

    def mix_block(t_off):
        block = mix_recv.at[tp_peer(t_off)]
        return block if t_off else block.at[pl.ds(0, n_ep - 1)]

    for t_off in range(0, n_tp, 2):
        block = mix_block(t_off)
        pltpu.make_async_copy(block, block, mix_rsem.at[t_off]).wait()
        block = mix_recv.at[tp_source(t_off)]
        pltpu.make_async_remote_copy(
            src_ref=block,
            dst_ref=block,
            send_sem=mix_ssem.at[t_off + 1],
            recv_sem=mix_rsem.at[t_off + 1],
            device_id=(ep, tp_peer(1)),
            device_id_type=MESH,
        ).start()
    def widen(t_off):
        source = tp_source(t_off)
        return jnp.concatenate([mix_recv[source, e].astype(F32) for e in range(n_ep)], axis=0)

    gain = as_row(ffn_gain)
    for source in range(n_tp):
        gain_parts[source] = gain[:, source * width : (source + 1) * width]
    wide = {t_off: widen(t_off) for t_off in range(0, n_tp, 2)}
    square = sum(jnp.sum(x * x, axis=-1, keepdims=True) for x in wide.values())
    for t_off in range(1, n_tp, 2):
        block = mix_block(t_off)
        pltpu.make_async_copy(block, block, mix_rsem.at[t_off]).wait()
    for t_off in range(1, n_tp, 2):
        wide[t_off] = widen(t_off)
        square = square + jnp.sum(wide[t_off] * wide[t_off], axis=-1, keepdims=True)
    factor = lax.rsqrt(square * (1.0 / depth) + NORM_EPSILON)
    inputs = {
        t_off: (x * factor * gain_parts[tp_source(t_off)]).astype(BF16)
        for t_off, x in wide.items()
    }

    def expand(weights, c):
        return sum(
            dot(
                x,
                weights[
                    pl.ds(pl.multiple_of(tp_source(t_off) * width, LANES), width),
                    c * chunk : (c + 1) * chunk,
                ],
            )
            for t_off, x in inputs.items()
        )

    loads["wg"].wait()
    loads["wu"].wait()
    chunks, _, chunk = hid_send.shape
    hid_copies = {}
    for c in range(chunks):
        gate = expand(wg, c)
        up = expand(wu, c)
        hidden = (gate / (1.0 + jnp.exp(-gate)) * up).astype(BF16)
        hid_send[c] = hidden
        for offset in range(n_tp - 1, 0, -1):
            hid_copies[c, offset] = pltpu.make_async_remote_copy(
                src_ref=hid_send.at[c],
                dst_ref=hid_recv.at[tp, c],
                send_sem=hid_ssem.at[c, offset],
                recv_sem=hid_rsem.at[c, offset],
                device_id=(ep, tp_peer(offset)),
                device_id_type=MESH,
            )
            hid_copies[c, offset].start()
    loads["wd"].wait()
    total = None
    for offset in range(n_tp):
        source = tp_source(offset)
        for c in range(chunks):
            if offset:
                hid_copies[c, offset].wait_recv()
                block = hid_recv[source, c]
            else:
                block = hid_send[c]
            start = pl.multiple_of(source * (chunk * chunks) + c * chunk, LANES)
            term = dot(block, wd[pl.ds(start, chunk), :])
            total = term if total is None else total + term
    for e in range(n_ep):
        ret_send[e] = total[e * rows : (e + 1) * rows, :].astype(BF16)

    def ret_copy(step):
        peer = ep_peer(step)
        return pltpu.make_async_remote_copy(
            src_ref=ret_send.at[peer],
            dst_ref=ret_recv.at[ep],
            send_sem=ret_ssem.at[0],
            recv_sem=ret_rsem.at[0],
            device_id=(peer, tp),
            device_id_type=MESH,
        )

    each(n_ep - 1, lambda step: ret_copy(far_first(step, 1)).start())
    ret_recv[ep] = ret_send[ep]

    row_index = lax.broadcasted_iota(jnp.int32, (rows, 1), 0)
    per_group = n_ep // GROUPS
    ids, shares = [], []
    for j in range(TOP):
        picked = jnp.zeros((rows, 1), jnp.int32)
        share = jnp.zeros((rows, 1), F32)
        for s in range(rows):
            picked = jnp.where(
                row_index == s, route_group[s] * per_group + route_expert[j, s], picked
            )
            share = jnp.where(row_index == s, route_weight[j, s], share)
        ids.append(picked)
        shares.append(share)
    for copy in q_copies + att_copies + list(hid_copies.values()):
        copy.wait_send()
    for t_off in range(n_tp):
        block = mix_block(t_off)
        pltpu.make_async_copy(block, block, mix_ssem.at[t_off]).wait()
    block = ret_recv.at[pl.ds(0, n_ep - 1)]
    pltpu.make_async_copy(block, block, ret_rsem.at[0]).wait()
    moe = None
    for picked, share in zip(ids, shares):
        result = jnp.zeros((rows, width), F32)
        for e in range(n_ep):
            result = jnp.where(picked == e, ret_recv[e].astype(F32), result)
        moe = share * result if moe is None else moe + share * result
    out[...] = (mix_send[...].astype(F32) + moe).astype(BF16)
    pltpu.make_async_copy(block, block, ret_ssem.at[0]).wait()


def on_device(
    tokens,
    attn_gain,
    ffn_gain,
    w_query,
    w_key,
    w_value,
    w_forget,
    forget_bias,
    w_out,
    cache_keys,
    cache_values,
    cache_logcum,
    cache_len,
    route_group,
    route_expert,
    route_weight,
    w_gate,
    w_up,
    w_down,
):
    n_ep, n_tp = lax.axis_size("ep"), lax.axis_size("tp")
    rows, depth = tokens.shape
    width = w_out.shape[1]
    part = w_gate.shape[2]
    chunk = min(part, 128)
    chunks = part // chunk
    every = n_ep * rows
    kv_width = KV_HEADS * HEAD
    hbm = pl.BlockSpec(memory_space=pl.ANY)
    small = (
        tokens,
        attn_gain.reshape(-1, LANES),
        ffn_gain.reshape(-1, LANES),
        forget_bias.reshape(1, QUERY_HEAD_COUNT),
    )
    scalars = (cache_len.reshape(1, 1), route_group, route_expert.T, route_weight.T)
    staged = (
        w_query,
        w_key,
        w_value,
        w_forget.T,
        w_out,
        cache_keys,
        cache_values,
        cache_logcum,
        w_gate,
        w_up,
        w_down,
    )
    dma = pltpu.SemaphoreType.DMA
    return pl.pallas_call(
        functools.partial(kernel, n_ep, n_tp),
        out_shape=pltpu.VMEM((rows, width), BF16),
        in_specs=[hbm] * (len(small) + len(scalars) + len(staged)),
        out_specs=pl.BlockSpec(memory_space=pltpu.VMEM),
        scratch_shapes=[pltpu.VMEM(a.shape, a.dtype) for a in small]
        + [pltpu.SMEM(a.shape, a.dtype) for a in scalars]
        + [pltpu.VMEM(a.shape[-2:], a.dtype) for a in staged]
        + [
            pltpu.VMEM((rows, 1, w_query.shape[1]), F32),
            pltpu.VMEM((n_tp, 1, w_query.shape[1]), F32),
            pltpu.VMEM((PER_KV, kv_width), BF16),
            pltpu.VMEM((n_tp, PER_KV, kv_width), BF16),
            pltpu.VMEM((kv_width // LANES, n_tp * PER_KV, LANES), F32),
            pltpu.VMEM((rows, width), BF16),
            pltpu.VMEM((n_tp, n_ep, rows, width), BF16),
            pltpu.VMEM((chunks, every, chunk), BF16),
            pltpu.VMEM((n_tp, chunks, every, chunk), BF16),
            pltpu.VMEM((n_ep, rows, width), BF16),
            pltpu.VMEM((n_ep, rows, width), BF16),
            dma((len(small) + len(scalars) + len(staged),)),
            dma((n_tp,)),
            dma((n_tp,)),
            dma((n_tp,)),
            dma((n_tp,)),
            dma((n_tp,)),
            dma((n_tp,)),
            dma((chunks, n_tp)),
            dma((chunks, n_tp)),
            dma((1,)),
            dma((1,)),
            pltpu.SemaphoreType.REGULAR((1 + max(1, (n_ep // 2 - 2).bit_length()),)),
            pltpu.VMEM((n_tp, 1, width), F32),
        ],
        compiler_params=pltpu.CompilerParams(
            collective_id=0, has_side_effects=True, vmem_limit_bytes=60 * 1024 * 1024
        ),
    )(
        *small,
        *scalars,
        *staged,
    )


def solution(mesh):
    placed = (
        P("ep", None),
        P(),
        P(),
        P(None, "tp"),
        P(),
        P(),
        P(),
        P(),
        P(None, "tp"),
        P(("ep", "tp"), None, None),
        P(("ep", "tp"), None, None),
        P(("ep", "tp"), None, None),
        P(("ep", "tp")),
        P("ep"),
        P("ep", None),
        P("ep", None),
        P("ep", None, "tp"),
        P("ep", None, "tp"),
        P("ep", None, "tp"),
    )
    return jax.shard_map(
        on_device, mesh=mesh, in_specs=placed, out_specs=P("ep", "tp"), check_vma=False
    )
```

profile of v0, /device:TPU:0, one launch (start us, length us, event | category | flops | bytes accessed | tf_op | source)
XLA Modules:
  0.0 26.2 jit_solution(2435187076069666040)
XLA Ops:
  0.7 24.9 %shard_map.181 = bf16[4,512]{1,0:T(4,128)(2,1)S(1)} custom-call(bf16[4,2048]{1,0:T(4,128)(2,1)} %tokens_hbm.1, bf16[16,128]{1,0:T(8,128)(2,1)} %bitcast.9, bf16[16,128]{1,0:T(8,128)(2,1)} %bitcast.10, f32[1,32]{1,0:T(1,128)} %bitcast.13, s32[1,1]{1,0:T(1,128)} %bitcast.7.cache_len_hbm, s32[4]{0:T(128)} %route_group_hbm.1, s32[2,4]{1,0:T(2,128)} %bitcast.11, ...), custom_call_target="tpu_custom_call" | custom-call | tf_op jit(solution)/shard_map/pallas_call | solution.py:549
  25.6 0.6 %copy.21 = bf16[4,512]{1,0:T(4,128)(2,1)} copy(bf16[4,512]{1,0:T(4,128)(2,1)S(1)} %shard_map.181) | data formatting | bytes 8192
where the time goes:
time: 26.4 us; the launch traced here: 26.2 us
  Pallas kernels  24.9 us (94%)
  between operations  0.66 us (2%)
  local copies, waits for them, and re-layouts  0.6 us (2%)
    pallas_call x1, Pallas kernels, on_device(): pl.pallas_call(functools.partial(kernel, n_ep, n_tp), out_shape=pltpu.VME...  24.9 us
    unnamed x1, local copies, waits for them, and re-layouts  0.6 us

commit v1 on v0

--- a/solution.py
+++ b/solution.py
@@ -14,6 +14,7 @@
 TOP = 2
 PER_KV = QUERY_HEAD_COUNT // KV_HEADS
 LANES = 128
+Q_PARTS = 4
 NORM_EPSILON = 1e-06
 MASKED_SCORE = -1e30
 F32 = jnp.float32
@@ -101,6 +102,7 @@
     att_rsem,
     mix_ssem,
     mix_rsem,
+    relay_ssem,
     hid_ssem,
     hid_rsem,
     ret_ssem,
@@ -128,6 +130,8 @@
     def far_first(step, skip):
         return skip + lax.rem(step + n_ep // 2 - 2 * skip, n_ep - skip)
 
+    q_part = wq.shape[0] // Q_PARTS
+    q_names = [f"wq{i}" for i in range(Q_PARTS)]
     loads = {}
     for index, (name, source, target) in enumerate(
         (
@@ -139,7 +143,10 @@
             ("route_group", route_group_hbm, route_group),
             ("route_expert", route_expert_hbm, route_expert),
             ("route_weight", route_weight_hbm, route_weight),
-            ("wq", wq_hbm, wq),
+            *[
+                (f"wq{i}", wq_hbm.at[pl.ds(i * q_part, q_part)], wq.at[pl.ds(i * q_part, q_part)])
+                for i in range(Q_PARTS)
+            ],
             ("wk", wk_hbm, wk),
             ("wv", wv_hbm, wv),
             ("wf", wf_hbm, wf),
@@ -154,31 +161,14 @@
     ):
         loads[name] = pltpu.make_async_copy(source, target, load_sem.at[index])
     small = ("ffn_gain", "forget_bias", "cache_len", "route_group", "route_expert", "route_weight")
-    for name in ("tokens", "attn_gain", "wq"):
+    for name in ("tokens", "attn_gain", *q_names):
         loads[name].start()
 
     barrier = pltpu.get_barrier_semaphore()
-    pair, pair_count = ep // 2, n_ep // 2
-
-    def signal_line(semaphore, distance):
-        for step in (-distance, distance):
-
-            @pl.when(jnp.logical_and(pair + step >= 0, pair + step < pair_count))
-            def _(step=step):
-                pl.semaphore_signal(
-                    semaphore, inc=1, device_id=(ep + 2 * step, tp), device_id_type=MESH
-                )
-
-    def line_count(distance):
-        before = (pair - distance >= 0).astype(jnp.int32)
-        return before + (pair + distance < pair_count).astype(jnp.int32)
-
+    leader = n_tp - 1
     for offset in range(1, n_tp):
         pl.semaphore_signal(barrier, inc=1, device_id=(ep, tp_peer(offset)), device_id_type=MESH)
-    other = pair * 2 + 1 - lax.rem(ep, 2)
-    pl.semaphore_signal(barrier, inc=1, device_id=(other, tp), device_id_type=MESH)
-    signal_line(barrier, 1)
-    for name in ("wk", "wv", "wf", *small, "logcum"):
+    for name in ("wk", "wv", "wf", *small, "logcum", "keys", "values", "wo", "wg", "wu", "wd"):
         loads[name].start()
 
     rows = tokens.shape[0]
@@ -191,13 +181,30 @@
     square = jnp.mean(stream * stream, axis=-1, keepdims=True)
     normed = (stream * lax.rsqrt(square + NORM_EPSILON) * as_row(attn_gain)).astype(BF16)
 
-    loads["wq"].wait()
-    query = dot(normed, wq[...]).astype(BF16).astype(F32)
-    for name in ("keys", "values", "wo", "wg", "wu", "wd"):
-        loads[name].start()
+    query = None
+    for i, name in enumerate(q_names):
+        loads[name].wait()
+        term = dot(normed[:, i * q_part : (i + 1) * q_part], wq[i * q_part : (i + 1) * q_part, :])
+        query = term if query is None else query + term
+    query = query.astype(BF16).astype(F32)
     for row in range(rows):
         q_send[row] = query[row : row + 1, :]
-    pl.semaphore_wait(barrier, n_tp + line_count(1))
+
+    @pl.when(tp != leader)
+    def _():
+        pl.semaphore_wait(barrier, n_tp - 1)
+        pl.semaphore_signal(near_sem.at[0], inc=1, device_id=(ep, leader), device_id_type=MESH)
+
+    @pl.when(tp == leader)
+    def _():
+        pl.semaphore_wait(near_sem.at[0], n_tp - 1)
+
+        def announce(step):
+            pl.semaphore_signal(
+                barrier, inc=1, device_id=(ep_peer(step + 1), leader), device_id_type=MESH
+            )
+
+        each(n_ep - 1, announce)
 
     def q_copy(offset):
         peer = tp_peer(offset)
@@ -215,20 +222,6 @@
         copy.start()
     q_recv[tp] = q_send[tp]
 
-    def spread(index):
-        if index == 1:
-            pl.semaphore_wait(near_sem.at[0], 1)
-        elif index:
-            pl.semaphore_wait(near_sem.at[index - 1], line_count(2 ** (index - 2)))
-        if index == 0:
-            pl.semaphore_signal(
-                near_sem.at[0], inc=1, device_id=(other, tp), device_id_type=MESH
-            )
-        elif index < near_sem.shape[0]:
-            signal_line(near_sem.at[index], 2 ** (index - 1))
-
-    spread(0)
-
     own = lax.broadcasted_iota(jnp.int32, (rows, 1), 0) == tp
 
     def own_row(values_all):
@@ -260,7 +253,6 @@
     bias = jnp.where(position < used, (latest + log_gate) - cum, MASKED_SCORE)
 
     loads["keys"].wait()
-    spread(1)
     for copy in q_copies:
         copy.wait_recv()
 
@@ -319,7 +311,18 @@
         copy.start()
     att_recv[tp] = attended
     loads["wo"].wait()
-    spread(2)
+
+    @pl.when(tp == leader)
+    def _():
+        pl.semaphore_wait(barrier, n_tp + n_ep - 2)
+        for offset in range(1, n_tp):
+            pl.semaphore_signal(
+                near_sem.at[1], inc=1, device_id=(ep, tp_peer(offset)), device_id_type=MESH
+            )
+
+    gain = as_row(ffn_gain)
+    for source in range(n_tp):
+        gain_parts[source] = gain[:, source * width : (source + 1) * width]
     for copy in att_copies:
         copy.wait_recv()
     for source in range(n_tp):
@@ -349,121 +352,153 @@
     mixed = (residual + projected).astype(BF16)
     mix_send[...] = mixed
 
-    for index in range(3, near_sem.shape[0] + 1):
-        spread(index)
-
-    def mix_copy(t_off, step):
+    @pl.when(tp != leader)
+    def _():
+        pl.semaphore_wait(near_sem.at[1], 1)
+
+    core = lax.rem(tp, 2)
+    batches = hid_send.shape[0]
+    span_ep = n_ep // batches
+    batch = ep // span_ep
+
+    def mix_copy(step, y_off, sem):
         return pltpu.make_async_remote_copy(
             src_ref=mix_send,
             dst_ref=mix_recv.at[tp, ep],
-            send_sem=mix_ssem.at[t_off],
-            recv_sem=mix_rsem.at[t_off],
-            device_id=(ep_peer(step), tp_peer(t_off)),
+            send_sem=mix_ssem.at[sem],
+            recv_sem=mix_rsem.at[tp, batch],
+            device_id=(ep_peer(step), lax.rem(tp // 2 + y_off, pairs) * 2 + 1),
             device_id_type=MESH,
         )
 
-    for t_off in range(0, n_tp, 2):
-        skip = 0 if t_off else 1
-        each(n_ep - skip, lambda step, t_off=t_off, skip=skip: mix_copy(t_off, far_first(step, skip)).start())
-    mix_recv[tp, ep] = mixed
-
-    def mix_block(t_off):
-        block = mix_recv.at[tp_peer(t_off)]
-        return block if t_off else block.at[pl.ds(0, n_ep - 1)]
-
-    for t_off in range(0, n_tp, 2):
-        block = mix_block(t_off)
-        pltpu.make_async_copy(block, block, mix_rsem.at[t_off]).wait()
-        block = mix_recv.at[tp_source(t_off)]
-        pltpu.make_async_remote_copy(
+    for y_off in range(pairs - 1, -1, -1):
+        each(n_ep - 1, lambda step, y_off=y_off: mix_copy(far_first(step, 1), y_off, y_off).start())
+    near_copies = [mix_copy(0, y_off, pairs + y_off) for y_off in range(pairs)]
+    for copy in near_copies[1:]:
+        copy.start()
+
+    @pl.when(core == 0)
+    def _():
+        near_copies[0].start()
+
+    @pl.when(core == 1)
+    def _():
+        pltpu.make_async_copy(mix_send, mix_recv.at[tp, ep], mix_rsem.at[tp, batch]).start()
+
+    def mix_source(k):
+        return lax.rem(tp // 2 + k % pairs, pairs) * 2 + (1 if k < pairs else 0)
+
+    def mix_block(k, b):
+        return mix_recv.at[mix_source(k), pl.ds(b * span_ep, span_ep)]
+
+    def mix_wait(k, b):
+        block = mix_block(k, b)
+        pltpu.make_async_copy(block, block, mix_rsem.at[mix_source(k), b]).wait()
+
+    def relay_copy(k, b):
+        block = mix_block(k, b)
+        return pltpu.make_async_remote_copy(
             src_ref=block,
             dst_ref=block,
-            send_sem=mix_ssem.at[t_off + 1],
-            recv_sem=mix_rsem.at[t_off + 1],
-            device_id=(ep, tp_peer(1)),
+            send_sem=relay_ssem.at[k, b],
+            recv_sem=mix_rsem.at[mix_source(k), b],
+            device_id=(ep, tp - core),
             device_id_type=MESH,
-        ).start()
-    def widen(t_off):
-        source = tp_source(t_off)
-        return jnp.concatenate([mix_recv[source, e].astype(F32) for e in range(n_ep)], axis=0)
-
-    gain = as_row(ffn_gain)
-    for source in range(n_tp):
-        gain_parts[source] = gain[:, source * width : (source + 1) * width]
-    wide = {t_off: widen(t_off) for t_off in range(0, n_tp, 2)}
-    square = sum(jnp.sum(x * x, axis=-1, keepdims=True) for x in wide.values())
-    for t_off in range(1, n_tp, 2):
-        block = mix_block(t_off)
-        pltpu.make_async_copy(block, block, mix_rsem.at[t_off]).wait()
-    for t_off in range(1, n_tp, 2):
-        wide[t_off] = widen(t_off)
-        square = square + jnp.sum(wide[t_off] * wide[t_off], axis=-1, keepdims=True)
-    factor = lax.rsqrt(square * (1.0 / depth) + NORM_EPSILON)
-    inputs = {
-        t_off: (x * factor * gain_parts[tp_source(t_off)]).astype(BF16)
-        for t_off, x in wide.items()
-    }
-
-    def expand(weights, c):
-        return sum(
-            dot(
-                x,
-                weights[
-                    pl.ds(pl.multiple_of(tp_source(t_off) * width, LANES), width),
-                    c * chunk : (c + 1) * chunk,
-                ],
+        )
+
+    chunks, _, chunk = hid_send.shape[1:]
+    hid_copies = {}
+
+    def expand(b):
+        gates, ups = [None] * chunks, [None] * chunks
+        square = None
+
+        @pl.when(core == 1)
+        def _():
+            for k in range(n_tp):
+                mix_wait(k, b)
+                relay_copy(k, b).start()
+
+        for k in range(n_tp):
+            @pl.when(core == 0)
+            def _(k=k):
+                mix_wait(k, b)
+
+            if b == 0 and k == 0:
+                loads["wg"].wait()
+                loads["wu"].wait()
+            source = mix_source(k)
+            wide = jnp.concatenate(
+                [mix_recv[source, b * span_ep + e].astype(F32) for e in range(span_ep)], axis=0
             )
-            for t_off, x in inputs.items()
-        )
-
-    loads["wg"].wait()
-    loads["wu"].wait()
-    chunks, _, chunk = hid_send.shape
-    hid_copies = {}
-    for c in range(chunks):
-        gate = expand(wg, c)
-        up = expand(wu, c)
-        hidden = (gate / (1.0 + jnp.exp(-gate)) * up).astype(BF16)
-        hid_send[c] = hidden
-        for offset in range(n_tp - 1, 0, -1):
-            hid_copies[c, offset] = pltpu.make_async_remote_copy(
-                src_ref=hid_send.at[c],
-                dst_ref=hid_recv.at[tp, c],
-                send_sem=hid_ssem.at[c, offset],
-                recv_sem=hid_rsem.at[c, offset],
-                device_id=(ep, tp_peer(offset)),
+            term = jnp.sum(wide * wide, axis=-1, keepdims=True)
+            square = term if square is None else square + term
+            scaled = (wide * gain_parts[source]).astype(BF16)
+            start = pl.multiple_of(source * width, LANES)
+            for c in range(chunks):
+                cols = slice(c * chunk, (c + 1) * chunk)
+                gate = dot(scaled, wg[pl.ds(start, width), cols])
+                up = dot(scaled, wu[pl.ds(start, width), cols])
+                gates[c] = gate if k == 0 else gates[c] + gate
+                ups[c] = up if k == 0 else ups[c] + up
+        factor = lax.rsqrt(square * (1.0 / depth) + NORM_EPSILON)
+        for c in range(chunks):
+            gate = gates[c] * factor
+            hidden = (gate / (1.0 + jnp.exp(-gate)) * (ups[c] * factor)).astype(BF16)
+            hid_send[b, c] = hidden
+            for offset in range(n_tp - 1, 0, -1):
+                hid_copies[b, c, offset] = pltpu.make_async_remote_copy(
+                    src_ref=hid_send.at[b, c],
+                    dst_ref=hid_recv.at[tp, b, c],
+                    send_sem=hid_ssem.at[b, c, offset],
+                    recv_sem=hid_rsem.at[b, c, offset],
+                    device_id=(ep, tp_peer(offset)),
+                    device_id_type=MESH,
+                )
+                hid_copies[b, c, offset].start()
+
+    def ret_copy(b, step):
+        peer = b * span_ep + lax.rem(ep + span_ep // 2 + step, span_ep)
+
+        @pl.when(peer != ep)
+        def _():
+            pltpu.make_async_remote_copy(
+                src_ref=ret_send.at[peer],
+                dst_ref=ret_recv.at[ep],
+                send_sem=ret_ssem.at[0],
+                recv_sem=ret_rsem.at[0],
+                device_id=(peer, tp),
                 device_id_type=MESH,
-            )
-            hid_copies[c, offset].start()
-    loads["wd"].wait()
-    total = None
-    for offset in range(n_tp):
-        source = tp_source(offset)
-        for c in range(chunks):
+            ).start()
+
+        @pl.when(peer == ep)
+        def _():
+            pltpu.make_async_copy(ret_send.at[ep], ret_recv.at[ep], ret_rsem.at[0]).start()
+
+    def contract(b):
+        if b == 0:
+            loads["wd"].wait()
+        order = [(offset, c) for offset in range(min(2, n_tp)) for c in range(chunks)]
+        order += [(offset, c) for c in range(chunks) for offset in range(2, n_tp)]
+        total = None
+        for offset, c in order:
+            source = tp_source(offset)
             if offset:
-                hid_copies[c, offset].wait_recv()
-                block = hid_recv[source, c]
+                hid_copies[b, c, offset].wait_recv()
+                block = hid_recv[source, b, c]
             else:
-                block = hid_send[c]
+                block = hid_send[b, c]
             start = pl.multiple_of(source * (chunk * chunks) + c * chunk, LANES)
             term = dot(block, wd[pl.ds(start, chunk), :])
             total = term if total is None else total + term
-    for e in range(n_ep):
-        ret_send[e] = total[e * rows : (e + 1) * rows, :].astype(BF16)
-
-    def ret_copy(step):
-        peer = ep_peer(step)
-        return pltpu.make_async_remote_copy(
-            src_ref=ret_send.at[peer],
-            dst_ref=ret_recv.at[ep],
-            send_sem=ret_ssem.at[0],
-            recv_sem=ret_rsem.at[0],
-            device_id=(peer, tp),
-            device_id_type=MESH,
-        )
-
-    each(n_ep - 1, lambda step: ret_copy(far_first(step, 1)).start())
-    ret_recv[ep] = ret_send[ep]
+        for e in range(span_ep):
+            ret_send[b * span_ep + e] = total[e * rows : (e + 1) * rows, :].astype(BF16)
+        each(span_ep, lambda step: ret_copy(b, step))
+
+    for b in range(batches):
+        expand(b)
+    for b in range(batches):
+        contract(b)
 
     row_index = lax.broadcasted_iota(jnp.int32, (rows, 1), 0)
     per_group = n_ep // GROUPS
@@ -480,11 +515,23 @@
         shares.append(share)
     for copy in q_copies + att_copies + list(hid_copies.values()):
         copy.wait_send()
-    for t_off in range(n_tp):
-        block = mix_block(t_off)
-        pltpu.make_async_copy(block, block, mix_ssem.at[t_off]).wait()
-    block = ret_recv.at[pl.ds(0, n_ep - 1)]
-    pltpu.make_async_copy(block, block, ret_rsem.at[0]).wait()
+    for y_off in range(pairs):
+        block = mix_recv.at[0, pl.ds(0, n_ep - 1)]
+        pltpu.make_async_copy(block, block, mix_ssem.at[y_off]).wait()
+    for copy in near_copies[1:]:
+        copy.wait_send()
+
+    @pl.when(core == 0)
+    def _():
+        near_copies[0].wait_send()
+
+    @pl.when(core == 1)
+    def _():
+        for b in range(batches):
+            for k in range(n_tp):
+                relay_copy(k, b).wait_send()
+
+    pltpu.make_async_copy(ret_recv, ret_recv, ret_rsem.at[0]).wait()
     moe = None
     for picked, share in zip(ids, shares):
         result = jnp.zeros((rows, width), F32)
@@ -492,6 +539,7 @@
             result = jnp.where(picked == e, ret_recv[e].astype(F32), result)
         moe = share * result if moe is None else moe + share * result
     out[...] = (mix_send[...].astype(F32) + moe).astype(BF16)
+    block = ret_recv.at[pl.ds(0, n_ep - 1)]
     pltpu.make_async_copy(block, block, ret_ssem.at[0]).wait()
 
 
@@ -520,7 +568,8 @@
     rows, depth = tokens.shape
     width = w_out.shape[1]
     part = w_gate.shape[2]
-    chunk = min(part, 128)
+    chunk = min(part, 256)
+    batches = 2 if n_ep % 2 == 0 else 1
     chunks = part // chunk
     every = n_ep * rows
     kv_width = KV_HEADS * HEAD
@@ -562,22 +611,23 @@
             pltpu.VMEM((kv_width // LANES, n_tp * PER_KV, LANES), F32),
             pltpu.VMEM((rows, width), BF16),
             pltpu.VMEM((n_tp, n_ep, rows, width), BF16),
-            pltpu.VMEM((chunks, every, chunk), BF16),
-            pltpu.VMEM((n_tp, chunks, every, chunk), BF16),
+            pltpu.VMEM((batches, chunks, every // batches, chunk), BF16),
+            pltpu.VMEM((n_tp, batches, chunks, every // batches, chunk), BF16),
             pltpu.VMEM((n_ep, rows, width), BF16),
             pltpu.VMEM((n_ep, rows, width), BF16),
-            dma((len(small) + len(scalars) + len(staged),)),
+            dma((len(small) + len(scalars) + len(staged) + Q_PARTS - 1,)),
             dma((n_tp,)),
             dma((n_tp,)),
             dma((n_tp,)),
             dma((n_tp,)),
             dma((n_tp,)),
-            dma((n_tp,)),
-            dma((chunks, n_tp)),
-            dma((chunks, n_tp)),
+            dma((n_tp, batches)),
+            dma((n_tp, batches)),
+            dma((batches, chunks, n_tp)),
+            dma((batches, chunks, n_tp)),
             dma((1,)),
             dma((1,)),
-            pltpu.SemaphoreType.REGULAR((1 + max(1, (n_ep // 2 - 2).bit_length()),)),
+            pltpu.SemaphoreType.REGULAR((2,)),
             pltpu.VMEM((n_tp, 1, width), F32),
         ],
         compiler_params=pltpu.CompilerParams(

time: 26.4 us -> 25.7 us (0.973)
  Pallas kernels: 24.9 us -> 24.2 us
    pallas_call x1, Pallas kernels: 24.9 us -> 24.2 us  [on_device(): pl.pallas_call(functools.partial(kernel, n_ep, n_tp), out_shape=pltpu.VME...]
where the time goes in v1:
time: 25.7 us; the launch traced here: 25.4 us
  Pallas kernels  24.2 us (94%)
  between operations  0.66 us (3%)
  local copies, waits for them, and re-layouts  0.6 us (2%)
    pallas_call x1, Pallas kernels, on_device(): pl.pallas_call(functools.partial(kernel, n_ep, n_tp), out_shape=pltpu.VME...  24.2 us
    unnamed x1, local copies, waits for them, and re-layouts  0.6 us

profile of v1, /device:TPU:0, one launch (start us, length us, event | category | flops | bytes accessed | tf_op | source)
XLA Modules:
  0.0 25.4 jit_solution(7448190482509485948)
XLA Ops:
  0.7 24.2 %shard_map.181 = bf16[4,512]{1,0:T(4,128)(2,1)S(1)} custom-call(bf16[4,2048]{1,0:T(4,128)(2,1)} %tokens_hbm.1, bf16[16,128]{1,0:T(8,128)(2,1)} %bitcast.9, bf16[16,128]{1,0:T(8,128)(2,1)} %bitcast.10, f32[1,32]{1,0:T(1,128)} %bitcast.13, s32[1,1]{1,0:T(1,128)} %bitcast.7.cache_len_hbm, s32[4]{0:T(128)} %route_group_hbm.1, s32[2,4]{1,0:T(2,128)} %bitcast.11, ...), custom_call_target="tpu_custom_call" | custom-call | tf_op jit(solution)/shard_map/pallas_call | solution.py:598
  24.8 0.6 %copy.21 = bf16[4,512]{1,0:T(4,128)(2,1)} copy(bf16[4,512]{1,0:T(4,128)(2,1)S(1)} %shard_map.181) | data formatting | bytes 8192

commit v2 on v1

--- a/solution.py
+++ b/solution.py
@@ -15,6 +15,7 @@
 PER_KV = QUERY_HEAD_COUNT // KV_HEADS
 LANES = 128
 Q_PARTS = 4
+SCORE_PARTS = 4
 NORM_EPSILON = 1e-06
 MASKED_SCORE = -1e30
 F32 = jnp.float32
@@ -96,16 +97,11 @@
     ret_send,
     ret_recv,
     load_sem,
-    q_ssem,
+    send_sem,
     q_rsem,
-    att_ssem,
     att_rsem,
-    mix_ssem,
     mix_rsem,
-    relay_ssem,
-    hid_ssem,
     hid_rsem,
-    ret_ssem,
     ret_rsem,
     near_sem,
     gain_parts,
@@ -132,35 +128,53 @@
 
     q_part = wq.shape[0] // Q_PARTS
     q_names = [f"wq{i}" for i in range(Q_PARTS)]
-    loads = {}
-    for index, (name, source, target) in enumerate(
-        (
-            ("tokens", tokens_hbm, tokens),
-            ("attn_gain", attn_gain_hbm, attn_gain),
-            ("ffn_gain", ffn_gain_hbm, ffn_gain),
-            ("forget_bias", forget_bias_hbm, forget_bias),
-            ("cache_len", cache_len_hbm, cache_len),
-            ("route_group", route_group_hbm, route_group),
-            ("route_expert", route_expert_hbm, route_expert),
-            ("route_weight", route_weight_hbm, route_weight),
-            *[
-                (f"wq{i}", wq_hbm.at[pl.ds(i * q_part, q_part)], wq.at[pl.ds(i * q_part, q_part)])
-                for i in range(Q_PARTS)
-            ],
-            ("wk", wk_hbm, wk),
-            ("wv", wv_hbm, wv),
-            ("wf", wf_hbm, wf),
-            ("logcum", logcum_hbm.at[0], logcum),
-            ("keys", keys_hbm.at[0], keys),
-            ("values", values_hbm.at[0], values),
-            ("wo", wo_hbm, wo),
-            ("wg", wg_hbm.at[0], wg),
-            ("wu", wu_hbm.at[0], wu),
-            ("wd", wd_hbm.at[0], wd),
-        )
-    ):
-        loads[name] = pltpu.make_async_copy(source, target, load_sem.at[index])
     small = ("ffn_gain", "forget_bias", "cache_len", "route_group", "route_expert", "route_weight")
+    groups = (
+        ("tokens", "attn_gain"),
+        *[(name,) for name in q_names],
+        ("wk",),
+        ("wv", "wf", *small, "logcum"),
+        ("keys", "values"),
+        ("wo", "wg", "wu", "wd"),
+    )
+    pieces = {
+        "tokens": (tokens_hbm, tokens),
+        "attn_gain": (attn_gain_hbm, attn_gain),
+        "ffn_gain": (ffn_gain_hbm, ffn_gain),
+        "forget_bias": (forget_bias_hbm, forget_bias),
+        "cache_len": (cache_len_hbm, cache_len),
+        "route_group": (route_group_hbm, route_group),
+        "route_expert": (route_expert_hbm, route_expert),
+        "route_weight": (route_weight_hbm, route_weight),
+        "wk": (wk_hbm, wk),
+        "wv": (wv_hbm, wv),
+        "wf": (wf_hbm, wf),
+        "logcum": (logcum_hbm.at[0], logcum),
+        "keys": (keys_hbm.at[0], keys),
+        "values": (values_hbm.at[0], values),
+        "wo": (wo_hbm, wo),
+        "wg": (wg_hbm.at[0], wg),
+        "wu": (wu_hbm.at[0], wu),
+        "wd": (wd_hbm.at[0], wd),
+    }
+    for i, name in enumerate(q_names):
+        part = pl.ds(i * q_part, q_part)
+        pieces[name] = (wq_hbm.at[part], wq.at[part])
+    loads = {
+        name: pltpu.make_async_copy(*pieces[name], load_sem.at[index])
+        for index, names in enumerate(groups)
+        for name in names
+    }
+
+    def loaded(first):
+        for names in groups:
+            if names[0] == first:
+                for name in names:
+                    loads[name].wait()
+
+    def drain(block, sem):
+        pltpu.make_async_copy(block, block, sem).wait()
+
     for name in ("tokens", "attn_gain", *q_names):
         loads[name].start()
 
@@ -168,15 +182,15 @@
     leader = n_tp - 1
     for offset in range(1, n_tp):
         pl.semaphore_signal(barrier, inc=1, device_id=(ep, tp_peer(offset)), device_id_type=MESH)
-    for name in ("wk", "wv", "wf", *small, "logcum", "keys", "values", "wo", "wg", "wu", "wd"):
-        loads[name].start()
+    for names in groups[1 + Q_PARTS :]:
+        for name in names:
+            loads[name].start()
 
     rows = tokens.shape[0]
     width = wo.shape[1]
     depth = tokens.shape[1]
     length = keys.shape[0]
-    loads["tokens"].wait()
-    loads["attn_gain"].wait()
+    loaded("tokens")
     stream = tokens[...].astype(F32)
     square = jnp.mean(stream * stream, axis=-1, keepdims=True)
     normed = (stream * lax.rsqrt(square + NORM_EPSILON) * as_row(attn_gain)).astype(BF16)
@@ -206,34 +220,38 @@
 
         each(n_ep - 1, announce)
 
-    def q_copy(offset):
-        peer = tp_peer(offset)
+    core = lax.rem(tp, 2)
+    pair = tp // 2
+    partner = tp + 1 - 2 * core
+
+    def far_pair(p):
+        return lax.rem(pair + p, pairs) * 2
+
+    peers = [far_pair(p) + d for p in range(1, pairs) for d in (0, 1)] + [partner]
+
+    def to_peer(source, target, peer, arrived):
         return pltpu.make_async_remote_copy(
-            src_ref=q_send.at[peer],
-            dst_ref=q_recv.at[tp],
-            send_sem=q_ssem.at[offset],
-            recv_sem=q_rsem.at[offset],
+            src_ref=source,
+            dst_ref=target,
+            send_sem=send_sem.at[0],
+            recv_sem=arrived,
             device_id=(ep, peer),
             device_id_type=MESH,
         )
 
-    q_copies = [q_copy(offset) for offset in range(1, n_tp)]
-    for copy in q_copies:
-        copy.start()
-    q_recv[tp] = q_send[tp]
+    for peer in peers:
+        to_peer(q_send.at[peer], q_recv.at[tp], peer, q_rsem.at[0]).start()
+    pltpu.make_async_copy(q_send.at[tp], q_recv.at[tp], q_rsem.at[0]).start()
 
     own = lax.broadcasted_iota(jnp.int32, (rows, 1), 0) == tp
 
     def own_row(values_all):
         return jnp.sum(jnp.where(own, values_all, 0.0), axis=0, keepdims=True)
 
-    loads["wk"].wait()
+    loaded("wk")
     key_new = own_row(dot(normed, wk[...])).astype(BF16).astype(F32)
-    loads["wv"].wait()
+    loaded("wv")
     value_new = own_row(dot(normed, wv[...])).astype(BF16).astype(F32)
-    loads["wf"].wait()
-    for name in small:
-        loads[name].wait()
     heads = QUERY_HEAD_COUNT
     gates = lax.dot_general(
         wf[...], normed, (((1,), (1,)), ((), ())), preferred_element_type=F32
@@ -247,14 +265,12 @@
     log_gate = jax.nn.log_sigmoid(gate_sum + bias_sum)
     used = cache_len[0, 0]
     position = lax.broadcasted_iota(jnp.int32, (1, length), 1)
-    loads["logcum"].wait()
     cum = logcum[...]
     latest = jnp.sum(jnp.where(position == used - 1, cum, 0.0), axis=1, keepdims=True)
     bias = jnp.where(position < used, (latest + log_gate) - cum, MASKED_SCORE)
 
-    loads["keys"].wait()
-    for copy in q_copies:
-        copy.wait_recv()
+    loaded("keys")
+    drain(q_recv, q_rsem.at[0])
 
     span = PER_KV * HEAD
     q_row = jnp.concatenate([q_recv[source] for source in range(n_tp)], axis=1)
@@ -274,20 +290,31 @@
         tiles = [zeros] * (KV_HEADS * HEAD // LANES)
         tiles[head * HEAD // LANES] = fold
         blocks.append(jnp.concatenate(tiles, axis=1))
-    q_heads = jnp.concatenate(blocks, axis=0)
-    scale = HEAD ** (-0.5)
-    own_score = jnp.sum(q_heads * key_new, axis=1, keepdims=True) * scale
-    score = lax.dot_general(
-        q_heads.astype(BF16), keys[...], (((1,), (1,)), ((), ())), preferred_element_type=F32
-    )
-    score = score * scale + bias
-    peak = jnp.maximum(jnp.max(score, axis=1, keepdims=True), own_score)
-    weight = jnp.exp(score - peak)
+    q_heads = jnp.concatenate(blocks, axis=0) * HEAD ** (-0.5)
+    own_score = jnp.sum(q_heads * key_new, axis=1, keepdims=True)
+    q_heads = q_heads.astype(BF16)
+    block = length // SCORE_PARTS
+    parts = []
+    for i in range(SCORE_PARTS):
+        used_rows = slice(i * block, (i + 1) * block)
+        score = lax.dot_general(
+            q_heads, keys[used_rows, :], (((1,), (1,)), ((), ())), preferred_element_type=F32
+        )
+        score = score + bias[:, used_rows]
+        top = jnp.max(score, axis=1, keepdims=True)
+        weight = jnp.exp(score - top)
+        total = jnp.sum(weight, axis=1, keepdims=True)
+        parts.append((top, total, dot(weight.astype(BF16), values[used_rows, :])))
+    peak = own_score
+    for top, _, _ in parts:
+        peak = jnp.maximum(peak, top)
     own_weight = jnp.exp(own_score - peak)
-    denominator = jnp.sum(weight, axis=1, keepdims=True) + own_weight
-    loads["values"].wait()
-    summed = dot(weight.astype(BF16), values[...])
-    summed = summed + own_weight.astype(BF16).astype(F32) * value_new
+    denominator = own_weight
+    summed = own_weight.astype(BF16).astype(F32) * value_new
+    for top, total, product in parts:
+        share = jnp.exp(top - peak)
+        denominator = denominator + share * total
+        summed = summed + share * product
     summed = summed / denominator
     kv_of = lax.broadcasted_iota(jnp.int32, (PER_KV, KV_HEADS * HEAD), 1) // HEAD
     folded = summed[:PER_KV]
@@ -296,21 +323,10 @@
     attended = folded.astype(BF16)
     att_send[...] = attended
 
-    def att_copy(offset):
-        return pltpu.make_async_remote_copy(
-            src_ref=att_send,
-            dst_ref=att_recv.at[tp],
-            send_sem=att_ssem.at[offset],
-            recv_sem=att_rsem.at[offset],
-            device_id=(ep, tp_peer(offset)),
-            device_id_type=MESH,
-        )
-
-    att_copies = [att_copy(offset) for offset in range(1, n_tp)]
-    for copy in att_copies[::-1]:
-        copy.start()
-    att_recv[tp] = attended
-    loads["wo"].wait()
+    for peer in peers:
+        to_peer(att_send, att_recv.at[tp], peer, att_rsem.at[0]).start()
+    pltpu.make_async_copy(att_send, att_recv.at[tp], att_rsem.at[0]).start()
+    loaded("wo")
 
     @pl.when(tp == leader)
     def _():
@@ -323,8 +339,7 @@
     gain = as_row(ffn_gain)
     for source in range(n_tp):
         gain_parts[source] = gain[:, source * width : (source + 1) * width]
-    for copy in att_copies:
-        copy.wait_recv()
+    drain(att_recv, att_rsem.at[0])
     for source in range(n_tp):
         arrived = att_recv[source].astype(F32)
         for tile in range(att_rows.shape[0]):
@@ -356,58 +371,38 @@
     def _():
         pl.semaphore_wait(near_sem.at[1], 1)
 
-    core = lax.rem(tp, 2)
-    batches = hid_send.shape[0]
+    batches, chunks, _, _, chunk = hid_recv.shape
     span_ep = n_ep // batches
     batch = ep // span_ep
-
-    def mix_copy(step, y_off, sem):
+    home = mix_recv.at[core, pair, ep]
+    home_sem = mix_rsem.at[core, batch]
+
+    def mix_copy(step, y_off):
         return pltpu.make_async_remote_copy(
             src_ref=mix_send,
-            dst_ref=mix_recv.at[tp, ep],
-            send_sem=mix_ssem.at[sem],
-            recv_sem=mix_rsem.at[tp, batch],
-            device_id=(ep_peer(step), lax.rem(tp // 2 + y_off, pairs) * 2 + 1),
+            dst_ref=home,
+            send_sem=send_sem.at[0],
+            recv_sem=home_sem,
+            device_id=(ep_peer(step), far_pair(y_off) + 1),
             device_id_type=MESH,
         )
 
     for y_off in range(pairs - 1, -1, -1):
-        each(n_ep - 1, lambda step, y_off=y_off: mix_copy(far_first(step, 1), y_off, y_off).start())
-    near_copies = [mix_copy(0, y_off, pairs + y_off) for y_off in range(pairs)]
-    for copy in near_copies[1:]:
-        copy.start()
+        each(n_ep - 1, lambda step, y_off=y_off: mix_copy(far_first(step, 1), y_off).start())
+    for y_off in range(1, pairs):
+        mix_copy(0, y_off).start()
 
     @pl.when(core == 0)
     def _():
-        near_copies[0].start()
+        mix_copy(0, 0).start()
 
     @pl.when(core == 1)
     def _():
-        pltpu.make_async_copy(mix_send, mix_recv.at[tp, ep], mix_rsem.at[tp, batch]).start()
-
-    def mix_source(k):
-        return lax.rem(tp // 2 + k % pairs, pairs) * 2 + (1 if k < pairs else 0)
-
-    def mix_block(k, b):
-        return mix_recv.at[mix_source(k), pl.ds(b * span_ep, span_ep)]
-
-    def mix_wait(k, b):
-        block = mix_block(k, b)
-        pltpu.make_async_copy(block, block, mix_rsem.at[mix_source(k), b]).wait()
-
-    def relay_copy(k, b):
-        block = mix_block(k, b)
-        return pltpu.make_async_remote_copy(
-            src_ref=block,
-            dst_ref=block,
-            send_sem=relay_ssem.at[k, b],
-            recv_sem=mix_rsem.at[mix_source(k), b],
-            device_id=(ep, tp - core),
-            device_id_type=MESH,
-        )
-
-    chunks, _, chunk = hid_send.shape[1:]
-    hid_copies = {}
+        pltpu.make_async_copy(mix_send, home, home_sem).start()
+
+    def mix_block(side, b):
+        return mix_recv.at[side, :, pl.ds(b * span_ep, span_ep)]
+
 
     def expand(b):
         gates, ups = [None] * chunks, [None] * chunks
@@ -415,21 +410,21 @@
 
         @pl.when(core == 1)
         def _():
-            for k in range(n_tp):
-                mix_wait(k, b)
-                relay_copy(k, b).start()
+            for side in (1, 0):
+                block = mix_block(side, b)
+                drain(block, mix_rsem.at[side, b])
+                to_peer(block, block, partner, mix_rsem.at[side, b]).start()
 
         for k in range(n_tp):
-            @pl.when(core == 0)
-            def _(k=k):
-                mix_wait(k, b)
-
-            if b == 0 and k == 0:
-                loads["wg"].wait()
-                loads["wu"].wait()
-            source = mix_source(k)
+            side, line = 1 - k // pairs, lax.rem(pair + k % pairs, pairs)
+            if k % pairs == 0:
+                @pl.when(core == 0)
+                def _(side=side):
+                    drain(mix_block(side, b), mix_rsem.at[side, b])
+
+            source = line * 2 + side
             wide = jnp.concatenate(
-                [mix_recv[source, b * span_ep + e].astype(F32) for e in range(span_ep)], axis=0
+                [mix_recv[side, line, b * span_ep + e].astype(F32) for e in range(span_ep)], axis=0
             )
             term = jnp.sum(wide * wide, axis=-1, keepdims=True)
             square = term if square is None else square + term
@@ -446,16 +441,9 @@
             gate = gates[c] * factor
             hidden = (gate / (1.0 + jnp.exp(-gate)) * (ups[c] * factor)).astype(BF16)
             hid_send[b, c] = hidden
-            for offset in range(n_tp - 1, 0, -1):
-                hid_copies[b, c, offset] = pltpu.make_async_remote_copy(
-                    src_ref=hid_send.at[b, c],
-                    dst_ref=hid_recv.at[tp, b, c],
-                    send_sem=hid_ssem.at[b, c, offset],
-                    recv_sem=hid_rsem.at[b, c, offset],
-                    device_id=(ep, tp_peer(offset)),
-                    device_id_type=MESH,
-                )
-                hid_copies[b, c, offset].start()
+            for peer in peers:
+                arrived = hid_rsem.at[b, 0 if peer is partner else 1 + c]
+                to_peer(hid_send.at[b, c], hid_recv.at[b, c, tp], peer, arrived).start()
 
     def ret_copy(b, step):
         peer = b * span_ep + lax.rem(ep + span_ep // 2 + step, span_ep)
@@ -465,7 +453,7 @@
             pltpu.make_async_remote_copy(
                 src_ref=ret_send.at[peer],
                 dst_ref=ret_recv.at[ep],
-                send_sem=ret_ssem.at[0],
+                send_sem=send_sem.at[1],
                 recv_sem=ret_rsem.at[0],
                 device_id=(peer, tp),
                 device_id_type=MESH,
@@ -476,21 +464,24 @@
             pltpu.make_async_copy(ret_send.at[ep], ret_recv.at[ep], ret_rsem.at[0]).start()
 
     def contract(b):
-        if b == 0:
-            loads["wd"].wait()
-        order = [(offset, c) for offset in range(min(2, n_tp)) for c in range(chunks)]
-        order += [(offset, c) for c in range(chunks) for offset in range(2, n_tp)]
         total = None
-        for offset, c in order:
-            source = tp_source(offset)
-            if offset:
-                hid_copies[b, c, offset].wait_recv()
-                block = hid_recv[source, b, c]
-            else:
-                block = hid_send[b, c]
+
+        def add(source, c, block):
+            nonlocal total
             start = pl.multiple_of(source * (chunk * chunks) + c * chunk, LANES)
             term = dot(block, wd[pl.ds(start, chunk), :])
             total = term if total is None else total + term
+
+        for c in range(chunks):
+            add(tp, c, hid_send[b, c])
+        drain(hid_recv.at[b, :, partner], hid_rsem.at[b, 0])
+        for c in range(chunks):
+            add(partner, c, hid_recv[b, c, partner])
+        for c in range(chunks):
+            drain(hid_recv.at[b, c, pl.ds(0, n_tp - 2)], hid_rsem.at[b, 1 + c])
+            for p in range(1, pairs):
+                for d in (1, 0):
+                    add(far_pair(p) + d, c, hid_recv[b, c, far_pair(p) + d])
         for e in range(span_ep):
             ret_send[b * span_ep + e] = total[e * rows : (e + 1) * rows, :].astype(BF16)
         each(span_ep, lambda step: ret_copy(b, step))
@@ -513,25 +504,21 @@
             share = jnp.where(row_index == s, route_weight[j, s], share)
         ids.append(picked)
         shares.append(share)
-    for copy in q_copies + att_copies + list(hid_copies.values()):
-        copy.wait_send()
-    for y_off in range(pairs):
-        block = mix_recv.at[0, pl.ds(0, n_ep - 1)]
-        pltpu.make_async_copy(block, block, mix_ssem.at[y_off]).wait()
-    for copy in near_copies[1:]:
-        copy.wait_send()
+    drain(q_recv.at[pl.ds(0, n_tp - 1)], send_sem.at[0])
+    drain(att_recv.at[pl.ds(0, n_tp - 1)], send_sem.at[0])
+    drain(mix_recv.at[0, :, pl.ds(0, n_ep - 1)], send_sem.at[0])
+    drain(mix_recv.at[0, pl.ds(0, pairs - 1), 0], send_sem.at[0])
+    drain(hid_recv.at[:, :, pl.ds(0, n_tp - 1)], send_sem.at[0])
 
     @pl.when(core == 0)
     def _():
-        near_copies[0].wait_send()
+        drain(mix_recv.at[0, 0, 0], send_sem.at[0])
 
     @pl.when(core == 1)
     def _():
-        for b in range(batches):
-            for k in range(n_tp):
-                relay_copy(k, b).wait_send()
-
-    pltpu.make_async_copy(ret_recv, ret_recv, ret_rsem.at[0]).wait()
+        drain(mix_recv, send_sem.at[0])
+
+    drain(ret_recv, ret_rsem.at[0])
     moe = None
     for picked, share in zip(ids, shares):
         result = jnp.zeros((rows, width), F32)
@@ -539,8 +526,7 @@
             result = jnp.where(picked == e, ret_recv[e].astype(F32), result)
         moe = share * result if moe is None else moe + share * result
     out[...] = (mix_send[...].astype(F32) + moe).astype(BF16)
-    block = ret_recv.at[pl.ds(0, n_ep - 1)]
-    pltpu.make_async_copy(block, block, ret_ssem.at[0]).wait()
+    drain(ret_recv.at[pl.ds(0, n_ep - 1)], send_sem.at[1])
 
 
 def on_device(
@@ -610,22 +596,17 @@
             pltpu.VMEM((n_tp, PER_KV, kv_width), BF16),
             pltpu.VMEM((kv_width // LANES, n_tp * PER_KV, LANES), F32),
             pltpu.VMEM((rows, width), BF16),
-            pltpu.VMEM((n_tp, n_ep, rows, width), BF16),
+            pltpu.VMEM((2, n_tp // 2, n_ep, rows, width), BF16),
             pltpu.VMEM((batches, chunks, every // batches, chunk), BF16),
-            pltpu.VMEM((n_tp, batches, chunks, every // batches, chunk), BF16),
+            pltpu.VMEM((batches, chunks, n_tp, every // batches, chunk), BF16),
             pltpu.VMEM((n_ep, rows, width), BF16),
             pltpu.VMEM((n_ep, rows, width), BF16),
-            dma((len(small) + len(scalars) + len(staged) + Q_PARTS - 1,)),
-            dma((n_tp,)),
-            dma((n_tp,)),
-            dma((n_tp,)),
-            dma((n_tp,)),
-            dma((n_tp,)),
-            dma((n_tp, batches)),
-            dma((n_tp, batches)),
-            dma((batches, chunks, n_tp)),
-            dma((batches, chunks, n_tp)),
+            dma((5 + Q_PARTS,)),
+            dma((2,)),
             dma((1,)),
+            dma((1,)),
+            dma((2, batches)),
+            dma((batches, 1 + chunks)),
             dma((1,)),
             pltpu.SemaphoreType.REGULAR((2,)),
             pltpu.VMEM((n_tp, 1, width), F32),

time: 25.7 us -> 25.1 us (0.977)
  Pallas kernels: 24.2 us -> 23.6 us
    pallas_call x1, Pallas kernels: 24.2 us -> 23.6 us  [on_device(): pl.pallas_call(functools.partial(kernel, n_ep, n_tp), out_shape=pltpu.VME...]
where the time goes in v2:
time: 25.1 us; the launch traced here: 24.9 us
  Pallas kernels  23.6 us (94%)
  between operations  0.66 us (3%)
  local copies, waits for them, and re-layouts  0.6 us (2%)
    pallas_call x1, Pallas kernels, on_device(): pl.pallas_call(functools.partial(kernel, n_ep, n_tp), out_shape=pltpu.VME...  23.6 us
    unnamed x1, local copies, waits for them, and re-layouts  0.6 us

profile of v2, /device:TPU:0, one launch (start us, length us, event | category | flops | bytes accessed | tf_op | source)
XLA Modules:
  0.0 24.9 jit_solution(9866386873184342710)
XLA Ops:
  0.7 23.6 %shard_map.181 = bf16[4,512]{1,0:T(4,128)(2,1)S(1)} custom-call(bf16[4,2048]{1,0:T(4,128)(2,1)} %tokens_hbm.1, bf16[16,128]{1,0:T(8,128)(2,1)} %bitcast.9, bf16[16,128]{1,0:T(8,128)(2,1)} %bitcast.10, f32[1,32]{1,0:T(1,128)} %bitcast.13, s32[1,1]{1,0:T(1,128)} %bitcast.7.cache_len_hbm, s32[4]{0:T(128)} %route_group_hbm.1, s32[2,4]{1,0:T(2,128)} %bitcast.11, ...), custom_call_target="tpu_custom_call" | custom-call | tf_op jit(solution)/shard_map/pallas_call | solution.py:584
  24.3 0.6 %copy.21 = bf16[4,512]{1,0:T(4,128)(2,1)} copy(bf16[4,512]{1,0:T(4,128)(2,1)S(1)} %shard_map.181) | data formatting | bytes 8192
